TPU v7x, 32 devices: a whole 2x2x4 slice. The times are simulated.
32 devices in a mesh: grp: 2 (over x), fs: 4 (over z), tp: 4 (over y, core).
Axes of the slice: x: 2, y: 2, z: 4, core: 2. Of those that a mesh axis runs over, the one named last changes fastest.
Arguments:
- tokens: bfloat16 [960, 2048], P(('grp', 'tp')), parts along dimension 0, may hold values from -60 to 60
- route_expert: int32 [960, 4], P(('grp', 'tp')), parts along dimension 0, may hold values from 0 to 31, all different within a row; in each aligned block of 120 rows (0 to 119, 120 to 239, ...) at most 16 rows name the same one
- route_weight: float32 [960, 4], P(('grp', 'tp')), parts along dimension 0, may hold values from 0.05 to 1
- norm_gain: float32 [2048], P('tp'), may hold values from 0.1 to 1.9
- gate_train: float32 [32, 2048, 2048], P(None, 'tp', 'fs'), may hold values from -8 to 8
- up_train: float32 [32, 2048, 2048], P(None, 'tp', 'fs'), may hold values from -8 to 8
- down_train: float32 [32, 2048, 2048], P(None, 'tp', 'fs'), may hold values from -0.013671875 to 0.013671875
Outputs:
- gate_serve: bfloat16 [64, 2048, 2048], P(('grp', 'tp'), None, 'fs'), parts along dimension 0
- up_serve: bfloat16 [64, 2048, 2048], P(('grp', 'tp'), None, 'fs'), parts along dimension 0
- down_serve: bfloat16 [64, 2048, 2048], P(('grp', 'tp'), None, 'fs'), parts along dimension 0
- mixed: bfloat16 [960, 2048], P(('grp', 'tp'), 'fs'), parts along dimension 0
There are 2 independent parts, one for each index of `grp`. A program takes and returns all parts, laid end to end along the dimension named above; an argument that names none is the same for every part. Nothing has to cross between parts.
Inputs may be any that keep to these rules, and one draw needn't show every extreme that they name: `route_expert`: each row names 4 different experts; the rows of one device name each expert at most 16 times.
All inputs are finite; a program needn't handle non-finite values.
Results may differ from a plain program's by a relative error of at most 0.0087.
Values may be sent and summed in bfloat16 or wider, within the bound.
A program may use at most 320 MiB of HBM per device.

v0:
```python
import jax
import jax.numpy as jnp
from jax import lax
from jax.sharding import PartitionSpec as P

EXPERTS = 32
TOP = 4
CAP = 16


def activate(gate_pre, up_pre):
    clamped = jnp.minimum(gate_pre, 7.0)
    bounded = jnp.clip(up_pre, -7.0, 7.0)
    return (clamped * jax.nn.sigmoid(1.702 * clamped) * (bounded + 1.0)).astype(jnp.bfloat16)


def local(tokens, route_expert, route_weight, norm_gain, gate_train, up_train, down_train):
    gate_local = (gate_train * norm_gain[None, :, None]).astype(jnp.bfloat16)
    up_local = (up_train * norm_gain[None, :, None]).astype(jnp.bfloat16)
    down_local = down_train.astype(jnp.bfloat16)
    gate_serve, up_serve, down_serve = (
        lax.all_to_all(gate_local, "tp", split_axis=0, concat_axis=1, tiled=True),
        lax.all_to_all(up_local, "tp", split_axis=0, concat_axis=1, tiled=True),
        lax.all_to_all(down_local, "tp", split_axis=0, concat_axis=1, tiled=True),
    )
    tp_count = lax.axis_size("tp")
    fs_count = lax.axis_size("fs")
    per_dev = EXPERTS // tp_count
    tok_rows = tokens.shape[0]
    floated = tokens.astype(jnp.float32)
    normed = (
        floated * lax.rsqrt(jnp.mean(floated * floated, axis=-1, keepdims=True) + 1e-06)
    ).astype(jnp.bfloat16)
    flat_expert = route_expert.reshape(-1)
    expert_ids = jnp.arange(EXPERTS, dtype=jnp.int32)
    onehot = (flat_expert[:, None] == expert_ids[None, :]).astype(jnp.int32)
    slot_rank = jnp.sum((jnp.cumsum(onehot, axis=0) - 1) * onehot, axis=1)
    slot_index = flat_expert * CAP + slot_rank
    slot_hit = slot_index[:, None] == jnp.arange(EXPERTS * CAP, dtype=jnp.int32)[None, :]
    placement = slot_hit.reshape(tok_rows, TOP, EXPERTS * CAP).astype(jnp.float32)
    scatter_mat = jnp.sum(placement, axis=1).astype(jnp.bfloat16)
    combine_mat = jnp.sum(placement * route_weight[:, :, None], axis=1)
    col_width = normed.shape[1] // fs_count
    my_block = lax.axis_index("fs")
    column_part = lax.dynamic_slice_in_dim(normed, my_block * col_width, col_width, 1)
    buffer = lax.dot_general(
        scatter_mat, column_part, (((0,), (0,)), ((), ())), preferred_element_type=jnp.float32
    )
    arrived = lax.all_to_all(
        buffer.astype(jnp.bfloat16).reshape(EXPERTS, CAP, column_part.shape[1]),
        "tp",
        split_axis=0,
        concat_axis=0,
        tiled=True,
    )
    arrived = arrived.reshape(tp_count, per_dev, CAP, col_width)
    block_in = lax.all_gather(arrived, "fs", axis=3, tiled=True)
    gate_part = jnp.einsum(
        "secd,edf->secf", block_in, gate_serve, preferred_element_type=jnp.float32
    )
    up_part = jnp.einsum("secd,edf->secf", block_in, up_serve, preferred_element_type=jnp.float32)
    hidden = activate(gate_part, up_part)
    expert_out = jnp.einsum(
        "secf,efd->secd",
        lax.all_gather(hidden, "fs", axis=3, tiled=True),
        down_serve,
        preferred_element_type=jnp.float32,
    ).astype(jnp.bfloat16)
    outgoing = expert_out.reshape(tp_count * per_dev, CAP, down_serve.shape[2])
    returned_rows = lax.all_to_all(outgoing, "tp", split_axis=0, concat_axis=0, tiled=True).reshape(
        EXPERTS * CAP, down_serve.shape[2]
    )
    mixed = jnp.dot(
        combine_mat, returned_rows.astype(jnp.float32), precision=lax.Precision.HIGHEST
    ).astype(jnp.bfloat16)
    return (gate_serve, up_serve, down_serve, mixed)


def solution(mesh):
    return jax.shard_map(
        local,
        mesh=mesh,
        in_specs=(
            P(("grp", "tp"), None),
            P(("grp", "tp"), None),
            P(("grp", "tp"), None),
            P("tp"),
            P(None, "tp", "fs"),
            P(None, "tp", "fs"),
            P(None, "tp", "fs"),
        ),
        out_specs=(
            P(("grp", "tp"), None, "fs"),
            P(("grp", "tp"), None, "fs"),
            P(("grp", "tp"), None, "fs"),
            P(("grp", "tp"), "fs"),
        ),
        check_vma=False,
    )
```

profile of v0, /device:TPU:0, one launch (start us, length us, event | category | flops | bytes accessed | tf_op | source)
XLA Modules:
  0.0 668.9 jit_solution(10352614119127516276)
XLA Ops:
  7.2 1.1 convert_element_type.44
  8.3 1.2 multiply_reduce_fusion
  9.5 0.8 copy.41
  10.3 0.1 eq.36
  10.5 1.2 reduce-window.6
  11.6 0.2 slice_reduce_fusion
  11.9 0.1 bitcast_bitcast_fusion
  12.0 0.1 reduce_sum.39
  12.1 0.1 copy.44
  12.2 0.7 multiply_add_fusion
  12.9 0.9 convert_reduce_fusion
  13.9 1.2 convolution_convert_fusion
  15.0 4.3 all-to-all-start.3
  19.3 33.2 %multiply_convert_fusion = (bf16[32,512,512]{2,1,0:T(8,128)(2,1)}, bf16[32,512,512]{2,1,0:T(8,128)(2,1)}) fusion(f32[32,512,512]{2,1,0:T(8,128)} %param.12, f32[512]{0:T(512)} %param.10, f32[32,512,512]{2,1,0:T(8,128)} %param.11), kind=kLoop, calls=%fused_computation | loop fusion | flops 33554432 | bytes 100665344 | tf_op jit(solution)/shard_map/convert_element_type | solution.py:19
  52.5 0.0 all-to-all-done.3
  52.5 194.1 %all_to_all.64 = bf16[32,512,512]{2,1,0:T(8,128)(2,1)} all-to-all(bf16[32,512,512]{2,1,0:T(8,128)(2,1)} %get-tuple-element.7), channel_id=1, replica_groups=mesh['grp'=2,'fs'=4,'tp'=4] {'tp'}, dimensions={0} | all-to-all | bytes 33554432 | tf_op jit(solution)/shard_map/all_to_all | solution.py:22
  246.6 7.1 %all-to-all-start.1 = ((bf16[32,512,512]{2,1,0:T(8,128)(2,1)}), bf16[32,512,512]{2,1,0:T(8,128)(2,1)}, u32[]{:S(2)}, u32[]{:S(2)}) async-start(bf16[32,512,512]{2,1,0:T(8,128)(2,1)} %get-tuple-element.6), calls=%async_computation.1 | async-start | bytes 33554432 | tf_op jit(solution)/shard_map/all_to_all | solution.py:23
  253.7 17.3 %convert_element_type.41 = bf16[32,512,512]{2,1,0:T(8,128)(2,1)} convert(f32[32,512,512]{2,1,0:T(8,128)} %param.13) | non-fusion elementwise | flops 8388608 | bytes 50331648 | tf_op jit(solution)/shard_map/convert_element_type | solution.py:20
  271.0 165.7 %all-to-all-done.1 = bf16[32,512,512]{2,1,0:T(8,128)(2,1)} async-done(((bf16[32,512,512]{2,1,0:T(8,128)(2,1)}), bf16[32,512,512]{2,1,0:T(8,128)(2,1)}, u32[]{:S(2)}, u32[]{:S(2)}) %all-to-all-start.1) | async-done | bytes 16777248 | tf_op jit(solution)/shard_map/all_to_all | solution.py:23
  436.7 7.0 %all-to-all-start.2 = ((bf16[32,512,512]{2,1,0:T(8,128)(2,1)}), bf16[32,512,512]{2,1,0:T(8,128)(2,1)}, u32[]{:S(2)}, u32[]{:S(2)}) async-start(bf16[32,512,512]{2,1,0:T(8,128)(2,1)} %convert_element_type.41), calls=%async_computation.2 | async-start | bytes 33554432 | tf_op jit(solution)/shard_map/all_to_all | solution.py:24
  443.6 0.0 all-gather.3.cloned.1.call-start
  443.7 0.8 copy.45
  444.5 0.0 all-gather.3.cloned.1.call-update
  444.6 0.0 all-gather.5.cloned.1.call-start
  444.6 13.8 %copy.38 = bf16[4,8,512,512]{3,2,0,1:T(8,128)(2,1)} copy(bf16[4,8,512,512]{3,2,1,0:T(8,128)(2,1)} %bitcast.59) | data formatting | bytes 33554432 | tf_op jit(solution)/shard_map/all_to_all | solution.py:22
  458.4 13.8 %copy.39 = bf16[4,8,512,512]{3,2,0,1:T(8,128)(2,1)} copy(bf16[4,8,512,512]{3,2,1,0:T(8,128)(2,1)} %bitcast.3) | data formatting | bytes 33554432 | tf_op jit(solution)/shard_map/all_to_all | solution.py:23
  472.3 22.4 %all-gather.3.cloned.1.call-done = bf16[4,8,16,2048]{3,2,0,1:T(8,128)(2,1)} async-done(((bf16[4,8,16,512]{3,2,0,1:T(8,128)(2,1)}), bf16[4,8,16,2048]{3,2,0,1:T(8,128)(2,1)}) %all-gather.3.cloned.1.call-update) | async-done | bytes 2097168 | tf_op jit(solution)/shard_map/all_gather | solution.py:57
  494.7 0.0 copy-start
  494.7 9.3 %fusion = f32[4,8,16,512]{3,2,0,1:T(8,128)S(1)} fusion(bf16[8,2048,512,1]{2,1,3,0:T(8,128)(2,1)} %bitcast.62, bf16[4,8,16,2048]{3,2,0,1:T(8,128)(2,1)} %all-gather.3.cloned.1.call-done), kind=kOutput, calls=%fused_computation.3 | convolution fusion | flops 1074003968 | bytes 19922944 | tf_op jit(solution)/shard_map/secd,edf->secf/dot_general | solution.py:58
  504.0 0.0 copy-done
  504.0 8.4 %fusion.4 = bf16[4,8,16,512]{3,2,0,1:T(8,128)(2,1)} fusion(bf16[8,2048,512,1]{2,1,3,0:T(8,128)(2,1)} %bitcast.64, bf16[4,8,16,2048]{3,2,0,1:T(8,128)(2,1)S(1)} %copy-done, f32[4,8,16,512]{3,2,0,1:T(8,128)S(1)} %fusion), kind=kOutput, calls=%fused_computation.10 | convolution fusion | flops 1076101120 | bytes 20447232 | tf_op jit(solution)/shard_map/secd,edf->secf/dot_general | solution.py:61
  512.4 0.0 all-gather.5.cloned.1.call-update
  512.4 114.3 %all-to-all-done.2 = bf16[32,512,512]{2,1,0:T(8,128)(2,1)} async-done(((bf16[32,512,512]{2,1,0:T(8,128)(2,1)}), bf16[32,512,512]{2,1,0:T(8,128)(2,1)}, u32[]{:S(2)}, u32[]{:S(2)}) %all-to-all-start.2) | async-done | bytes 16777248 | tf_op jit(solution)/shard_map/all_to_all | solution.py:24
  626.7 13.8 %copy.40 = bf16[4,8,512,512]{3,2,0,1:T(8,128)(2,1)} copy(bf16[4,8,512,512]{3,2,1,0:T(8,128)(2,1)} %bitcast.6) | data formatting | bytes 33554432 | tf_op jit(solution)/shard_map/all_to_all | solution.py:24
  640.5 0.0 all-gather.5.cloned.1.call-done
  640.5 9.3 %fusion.5 = bf16[4,8,16,512]{3,2,0,1:T(8,128)(2,1)S(1)} fusion(bf16[4,8,16,2048]{3,2,0,1:T(8,128)(2,1)} %all-gather.5.cloned.1.call-done, bf16[8,2048,512,1]{2,1,3,0:T(8,128)(2,1)} %bitcast.60), kind=kOutput, calls=%fused_computation.11 | convolution fusion | flops 1074003968 | bytes 19398656 | tf_op jit(solution)/shard_map/secf,efd->secd/dot_general | solution.py:63
  649.8 11.2 %all_to_all.65 = bf16[32,16,512]{2,1,0:T(8,128)(2,1)S(1)} all-to-all(bf16[32,16,512]{2,1,0:T(8,128)(2,1)S(1)} %bitcast.68), channel_id=1, replica_groups=mesh['grp'=2,'fs'=4,'tp'=4] {'tp'}, dimensions={0} | all-to-all | bytes 1048576 | tf_op jit(solution)/shard_map/all_to_all | solution.py:70
  661.0 1.0 convolution_convert_fusion.2
  (7 shorter events, 0.1 us)
Async XLA Ops:
  15.0 37.4 %all-to-all-start.3 = ((bf16[32,16,512]{2,1,0:T(8,128)(2,1)}), bf16[32,16,512]{2,1,0:T(8,128)(2,1)S(1)}, u32[]{:S(2)}, u32[]{:S(2)}) async-start(bf16[32,16,512]{2,1,0:T(8,128)(2,1)} %bitcast.13), calls=%async_computation.3 | async-start | bytes 1048576 | tf_op jit(solution)/shard_map/all_to_all | solution.py:49
  246.6 190.1 %all-to-all-start.1 = ((bf16[32,512,512]{2,1,0:T(8,128)(2,1)}), bf16[32,512,512]{2,1,0:T(8,128)(2,1)}, u32[]{:S(2)}, u32[]{:S(2)}) async-start(bf16[32,512,512]{2,1,0:T(8,128)(2,1)} %get-tuple-element.6), calls=%async_computation.1 | async-start | bytes 33554432 | tf_op jit(solution)/shard_map/all_to_all | solution.py:23
  436.7 190.0 %all-to-all-start.2 = ((bf16[32,512,512]{2,1,0:T(8,128)(2,1)}), bf16[32,512,512]{2,1,0:T(8,128)(2,1)}, u32[]{:S(2)}, u32[]{:S(2)}) async-start(bf16[32,512,512]{2,1,0:T(8,128)(2,1)} %convert_element_type.41), calls=%async_computation.2 | async-start | bytes 33554432 | tf_op jit(solution)/shard_map/all_to_all | solution.py:24
  443.6 51.0 %all-gather.3.cloned.1.call-start = ((), (), s32[]{:S(2)}) async-start(), calls=%async_computation.5 | async-start | bytes 2621440 | tf_op jit(solution)/shard_map/all_gather | solution.py:57
  444.6 195.9 %all-gather.5.cloned.1.call-start = ((), (), s32[]{:S(2)}) async-start(), calls=%async_computation.6 | async-start | bytes 2621440 | tf_op jit(solution)/shard_map/all_gather | solution.py:65
  494.7 9.3 %copy-start = (bf16[4,8,16,2048]{3,2,0,1:T(8,128)(2,1)S(1)}, bf16[4,8,16,2048]{3,2,0,1:T(8,128)(2,1)}, u32[]{:S(2)}) copy-start(bf16[4,8,16,2048]{3,2,0,1:T(8,128)(2,1)} %all-gather.3.cloned.1.call-done) | copy-start | bytes 6291460
Sparse Core Ops, SparseCore 0:
  446.6 48.0 all-gather.2
  512.5 44.4 all-gather.4
where the time goes:
time: 670 us; the launch traced here: 669 us
  waiting for transfers between devices  302 us (45%)
  blocking collectives  205 us (31%)
  other arithmetic  55.9 us (8%)
  local copies, waits for them, and re-layouts  43.6 us (7%)
  matrix products  29.2 us (4%)
  starting transfers between devices  18.4 us (3%)
  between operations  14.2 us (2%)
    all_to_all x1, blocking collectives, local(): lax.all_to_all(gate_local, 'tp', split_axis=0, concat_axis=1, tiled=True)  194 us
    all_to_all x1, waiting for transfers between devices, local(): lax.all_to_all(up_local, 'tp', split_axis=0, concat_axis=1, tiled=True)  166 us
    all_to_all x1, waiting for transfers between devices, local(): lax.all_to_all(down_local, 'tp', split_axis=0, concat_axis=1, tiled=True)  114 us
    convert_element_type x1, other arithmetic, local(): up_local = (up_train * norm_gain[None, :, None]).astype(jnp.bfloat16)  33.2 us
    all_gather x1, waiting for transfers between devices, local(): block_in = lax.all_gather(arrived, 'fs', axis=3, tiled=True)  22.4 us
    convert_element_type x1, other arithmetic, local(): down_local = down_train.astype(jnp.bfloat16)  17.3 us
    all_to_all x1, local copies, waits for them, and re-layouts, local(): lax.all_to_all(gate_local, 'tp', split_axis=0, concat_axis=1, tiled=True)  13.8 us
    all_to_all x1, local copies, waits for them, and re-layouts, local(): lax.all_to_all(up_local, 'tp', split_axis=0, concat_axis=1, tiled=True)  13.8 us
  transfers between devices with their start and end apart: 5, of which 3 were waited for; matrix products, arithmetic and copies ran while one was open for 17% of the time, Pallas kernels for 0%

commit v1 on v0

--- a/solution.py
+++ b/solution.py
@@ -6,6 +6,15 @@
 EXPERTS = 32
 TOP = 4
 CAP = 16
+
+
+def try_all_orders(array_here, dim_at, dimension_no):
+    return jnp.concatenate(
+        lax.all_to_all(
+            jnp.stack(jnp.split(array_here, lax.axis_size("tp"), dim_at), 0), "tp", 0, 0
+        ),
+        dimension_no,
+    )
 
 
 def activate(gate_pre, up_pre):
@@ -21,7 +30,7 @@
     gate_serve, up_serve, down_serve = (
         lax.all_to_all(gate_local, "tp", split_axis=0, concat_axis=1, tiled=True),
         lax.all_to_all(up_local, "tp", split_axis=0, concat_axis=1, tiled=True),
-        lax.all_to_all(down_local, "tp", split_axis=0, concat_axis=1, tiled=True),
+        try_all_orders(down_local, 0, 1),
     )
     tp_count = lax.axis_size("tp")
     fs_count = lax.axis_size("fs")

time: 670 us -> 669 us (level)
  waiting for transfers between devices: 302 us -> 288 us
  other arithmetic: 55.9 us -> 64.3 us
    all_to_all x1, waiting for transfers between devices: 166 us -> 151 us  [local(): lax.all_to_all(up_local, 'tp', split_axis=0, concat_axis=1, tiled=True)]
    another operation x4 -> x5, other arithmetic: 1.3 us -> 15.1 us  [the longest x1 13.8 us: try_all_orders(): jnp.stack(jnp.split(array_here, lax.axis_size('tp'), dim_at), 0)]
    all_to_all x1 -> x0, local copies, waits for them, and re-layouts: 13.8 us -> none  [local(): lax.all_to_all(down_local, 'tp', split_axis=0, concat_axis=1, tiled=True)]
    reshape x0 -> x1, local copies, waits for them, and re-layouts: none -> 13.8 us  [try_all_orders(): jnp.concatenate(lax.all_to_all(jnp.stack(jnp.split(array_here, lax.axis_s...]
  transfers between devices with their start and end apart: 5 -> 5, of which waited for: 3 -> 3; matrix products, arithmetic and copies ran while one was open for 17% -> 19% of each run, Pallas kernels for 0% -> 0%
where the time goes in v1:
time: 669 us; the launch traced here: 667 us
  waiting for transfers between devices  288 us (43%)
  blocking collectives  205 us (31%)
  other arithmetic  64.3 us (10%)
  local copies, waits for them, and re-layouts  49.7 us (7%)
  matrix products  27.7 us (4%)
  starting transfers between devices  18.4 us (3%)
  between operations  14.2 us (2%)
    all_to_all x1, blocking collectives, local(): lax.all_to_all(gate_local, 'tp', split_axis=0, concat_axis=1, tiled=True)  194 us
    all_to_all x1, waiting for transfers between devices, local(): lax.all_to_all(up_local, 'tp', split_axis=0, concat_axis=1, tiled=True)  151 us
    all_to_all x1, waiting for transfers between devices, try_all_orders(): lax.all_to_all(jnp.stack(jnp.split(array_here, lax.axis_size('tp'), dim_a...  114 us
    convert_element_type x1, other arithmetic, local(): up_local = (up_train * norm_gain[None, :, None]).astype(jnp.bfloat16)  33.2 us
    all_gather x1, waiting for transfers between devices, local(): block_in = lax.all_gather(arrived, 'fs', axis=3, tiled=True)  22.4 us
    all_to_all x1, local copies, waits for them, and re-layouts, local(): lax.all_to_all(gate_local, 'tp', split_axis=0, concat_axis=1, tiled=True)  13.8 us
    another operation x1, other arithmetic, try_all_orders(): jnp.stack(jnp.split(array_here, lax.axis_size('tp'), dim_at), 0)  13.8 us
    all_to_all x1, local copies, waits for them, and re-layouts, local(): lax.all_to_all(up_local, 'tp', split_axis=0, concat_axis=1, tiled=True)  13.8 us
  transfers between devices with their start and end apart: 5, of which 3 were waited for; matrix products, arithmetic and copies ran while one was open for 19% of the time, Pallas kernels for 0%

profile of v1, /device:TPU:0, one launch (start us, length us, event | category | flops | bytes accessed | tf_op | source)
XLA Modules:
  0.0 667.4 jit_solution(1817405561818624156)
XLA Ops:
  7.2 1.1 convert_element_type.44
  8.3 1.2 multiply_reduce_fusion
  9.5 0.8 copy.41
  10.3 0.1 eq.36
  10.5 1.2 reduce-window.6
  11.6 0.2 slice_reduce_fusion
  11.9 0.1 bitcast_bitcast_fusion
  12.0 0.1 reduce_sum.39
  12.1 0.1 copy.44
  12.2 0.7 multiply_add_fusion
  12.9 0.9 convert_reduce_fusion
  13.9 1.2 convolution_convert_fusion
  15.0 4.3 all-to-all-start.3
  19.3 33.2 %multiply_convert_fusion = (bf16[32,512,512]{2,1,0:T(8,128)(2,1)}, bf16[32,512,512]{2,1,0:T(8,128)(2,1)}) fusion(f32[32,512,512]{2,1,0:T(8,128)} %param.12, f32[512]{0:T(512)} %param.10, f32[32,512,512]{2,1,0:T(8,128)} %param.11), kind=kLoop, calls=%fused_computation | loop fusion | flops 33554432 | bytes 100665344 | tf_op jit(solution)/shard_map/convert_element_type | solution.py:28
  52.5 0.0 all-to-all-done.3
  52.5 194.1 %all_to_all.51 = bf16[32,512,512]{2,1,0:T(8,128)(2,1)} all-to-all(bf16[32,512,512]{2,1,0:T(8,128)(2,1)} %get-tuple-element.11), channel_id=1, replica_groups=mesh['grp'=2,'fs'=4,'tp'=4] {'tp'}, dimensions={0} | all-to-all | bytes 33554432 | tf_op jit(solution)/shard_map/all_to_all | solution.py:31
  246.6 7.0 %all-to-all-start.1 = ((bf16[32,512,512]{2,1,0:T(8,128)(2,1)}), bf16[32,512,512]{2,1,0:T(8,128)(2,1)}, u32[]{:S(2)}, u32[]{:S(2)}) async-start(bf16[32,512,512]{2,1,0:T(8,128)(2,1)} %get-tuple-element.10), calls=%async_computation.1 | async-start | bytes 33554432 | tf_op jit(solution)/shard_map/all_to_all | solution.py:32
  253.5 11.9 %convert_element_type.41 = bf16[32,512,512]{2,1,0:T(8,128)(2,1)S(1)} convert(f32[32,512,512]{2,1,0:T(8,128)} %param.13) | non-fusion elementwise | flops 8388608 | bytes 50331648 | tf_op jit(solution)/shard_map/convert_element_type | solution.py:29
  265.5 6.1 slice_bitcast_fusion.3
  271.5 13.8 %pad_maximum_fusion = bf16[4,8,512,512]{3,2,1,0:T(8,128)(2,1)} fusion(bf16[1,8,512,512]{3,2,1,0:T(8,128)(2,1)} %get-tuple-element.7, bf16[1,8,512,512]{3,2,1,0:T(8,128)(2,1)} %get-tuple-element.8, bf16[1,8,512,512]{3,2,1,0:T(8,128)(2,1)} %get-tuple-element.9, bf16[1,8,512,512]{3,2,1,0:T(8,128)(2,1)} %get-tuple-element.6), kind=kLoop, calls=%fused_computation.2 | loop fusion | flops 25165824 | bytes 33554432 | tf_op jit(solution)/shard_map/stack | solution.py:14
  285.4 151.2 %all-to-all-done.1 = bf16[32,512,512]{2,1,0:T(8,128)(2,1)} async-done(((bf16[32,512,512]{2,1,0:T(8,128)(2,1)}), bf16[32,512,512]{2,1,0:T(8,128)(2,1)}, u32[]{:S(2)}, u32[]{:S(2)}) %all-to-all-start.1) | async-done | bytes 16777248 | tf_op jit(solution)/shard_map/all_to_all | solution.py:32
  436.5 7.1 %all-to-all-start.2 = ((bf16[4,8,512,512]{3,2,1,0:T(8,128)(2,1)}), bf16[4,8,512,512]{3,2,1,0:T(8,128)(2,1)}, u32[]{:S(2)}, u32[]{:S(2)}) async-start(bf16[4,8,512,512]{3,2,1,0:T(8,128)(2,1)} %pad_maximum_fusion), calls=%async_computation.2 | async-start | bytes 33554432 | tf_op jit(solution)/shard_map/all_to_all | solution.py:13
  443.6 0.0 all-gather.3.cloned.1.call-start
  443.7 0.8 copy.45
  444.5 0.0 all-gather.3.cloned.1.call-update
  444.5 0.0 all-gather.5.cloned.1.call-start
  444.6 13.8 %copy.38 = bf16[4,8,512,512]{3,2,0,1:T(8,128)(2,1)} copy(bf16[4,8,512,512]{3,2,1,0:T(8,128)(2,1)} %bitcast.65) | data formatting | bytes 33554432 | tf_op jit(solution)/shard_map/all_to_all | solution.py:31
  458.4 13.8 %copy.39 = bf16[4,8,512,512]{3,2,0,1:T(8,128)(2,1)} copy(bf16[4,8,512,512]{3,2,1,0:T(8,128)(2,1)} %bitcast.3) | data formatting | bytes 33554432 | tf_op jit(solution)/shard_map/all_to_all | solution.py:32
  472.2 22.4 %all-gather.3.cloned.1.call-done = bf16[4,8,16,2048]{3,2,0,1:T(8,128)(2,1)} async-done(((bf16[4,8,16,512]{3,2,0,1:T(8,128)(2,1)}), bf16[4,8,16,2048]{3,2,0,1:T(8,128)(2,1)}) %all-gather.3.cloned.1.call-update) | async-done | bytes 2097168 | tf_op jit(solution)/shard_map/all_gather | solution.py:66
  494.7 0.0 copy-start
  494.7 9.3 %fusion = f32[4,8,16,512]{3,2,0,1:T(8,128)S(1)} fusion(bf16[8,2048,512,1]{2,1,3,0:T(8,128)(2,1)} %bitcast.66, bf16[4,8,16,2048]{3,2,0,1:T(8,128)(2,1)} %all-gather.3.cloned.1.call-done), kind=kOutput, calls=%fused_computation.8 | convolution fusion | flops 1074003968 | bytes 19922944 | tf_op jit(solution)/shard_map/secd,edf->secf/dot_general | solution.py:67
  504.0 0.0 copy-done
  504.0 8.4 %fusion.4 = bf16[4,8,16,512]{3,2,0,1:T(8,128)(2,1)} fusion(bf16[8,2048,512,1]{2,1,3,0:T(8,128)(2,1)} %bitcast.68, bf16[4,8,16,2048]{3,2,0,1:T(8,128)(2,1)S(1)} %copy-done, f32[4,8,16,512]{3,2,0,1:T(8,128)S(1)} %fusion), kind=kOutput, calls=%fused_computation.15 | convolution fusion | flops 1076101120 | bytes 20447232 | tf_op jit(solution)/shard_map/secd,edf->secf/dot_general | solution.py:70
  512.3 0.0 all-gather.5.cloned.1.call-update
  512.4 114.3 %all-to-all-done.2 = bf16[4,8,512,512]{3,2,1,0:T(8,128)(2,1)} async-done(((bf16[4,8,512,512]{3,2,1,0:T(8,128)(2,1)}), bf16[4,8,512,512]{3,2,1,0:T(8,128)(2,1)}, u32[]{:S(2)}, u32[]{:S(2)}) %all-to-all-start.2) | async-done | bytes 16777248 | tf_op jit(solution)/shard_map/all_to_all | solution.py:13
  626.6 13.8 %copy.40 = bf16[8,4,512,512]{3,2,1,0:T(8,128)(2,1)} copy(bf16[8,4,512,512]{3,2,0,1:T(8,128)(2,1)} %bitcast.10) | data formatting | bytes 33554432 | tf_op jit(solution)/shard_map/reshape | solution.py:12
  640.4 0.0 all-gather.5.cloned.1.call-done
  640.4 7.9 %fusion.5 = bf16[4,8,16,512]{3,2,0,1:T(8,128)(2,1)S(1)} fusion(bf16[8,2048,512,1]{2,1,3,0:T(8,128)(2,1)} %bitcast.70, bf16[4,8,16,2048]{3,2,0,1:T(8,128)(2,1)} %all-gather.5.cloned.1.call-done), kind=kOutput, calls=%fused_computation.16 | convolution fusion | flops 1074003968 | bytes 19398656 | tf_op jit(solution)/shard_map/secf,efd->secd/dot_general | solution.py:72
  648.4 11.2 %all_to_all.52 = bf16[32,16,512]{2,1,0:T(8,128)(2,1)S(1)} all-to-all(bf16[32,16,512]{2,1,0:T(8,128)(2,1)S(1)} %bitcast.74), channel_id=1, replica_groups=mesh['grp'=2,'fs'=4,'tp'=4] {'tp'}, dimensions={0} | all-to-all | bytes 1048576 | tf_op jit(solution)/shard_map/all_to_all | solution.py:79
  659.6 1.0 convolution_convert_fusion.2
  (7 shorter events, 0.1 us)
Async XLA Ops:
  15.0 37.4 %all-to-all-start.3 = ((bf16[32,16,512]{2,1,0:T(8,128)(2,1)}), bf16[32,16,512]{2,1,0:T(8,128)(2,1)S(1)}, u32[]{:S(2)}, u32[]{:S(2)}) async-start(bf16[32,16,512]{2,1,0:T(8,128)(2,1)} %bitcast.18), calls=%async_computation.3 | async-start | bytes 1048576 | tf_op jit(solution)/shard_map/all_to_all | solution.py:58
  246.6 190.0 %all-to-all-start.1 = ((bf16[32,512,512]{2,1,0:T(8,128)(2,1)}), bf16[32,512,512]{2,1,0:T(8,128)(2,1)}, u32[]{:S(2)}, u32[]{:S(2)}) async-start(bf16[32,512,512]{2,1,0:T(8,128)(2,1)} %get-tuple-element.10), calls=%async_computation.1 | async-start | bytes 33554432 | tf_op jit(solution)/shard_map/all_to_all | solution.py:32
  436.5 190.1 %all-to-all-start.2 = ((bf16[4,8,512,512]{3,2,1,0:T(8,128)(2,1)}), bf16[4,8,512,512]{3,2,1,0:T(8,128)(2,1)}, u32[]{:S(2)}, u32[]{:S(2)}) async-start(bf16[4,8,512,512]{3,2,1,0:T(8,128)(2,1)} %pad_maximum_fusion), calls=%async_computation.2 | async-start | bytes 33554432 | tf_op jit(solution)/shard_map/all_to_all | solution.py:13
  443.6 51.0 %all-gather.3.cloned.1.call-start = ((), (), s32[]{:S(2)}) async-start(), calls=%async_computation.5 | async-start | bytes 2621440 | tf_op jit(solution)/shard_map/all_gather | solution.py:66
  444.5 195.9 %all-gather.5.cloned.1.call-start = ((), (), s32[]{:S(2)}) async-start(), calls=%async_computation.6 | async-start | bytes 2621440 | tf_op jit(solution)/shard_map/all_gather | solution.py:74
  494.7 9.3 %copy-start = (bf16[4,8,16,2048]{3,2,0,1:T(8,128)(2,1)S(1)}, bf16[4,8,16,2048]{3,2,0,1:T(8,128)(2,1)}, u32[]{:S(2)}) copy-start(bf16[4,8,16,2048]{3,2,0,1:T(8,128)(2,1)} %all-gather.3.cloned.1.call-done) | copy-start | bytes 6291460
Sparse Core Ops, SparseCore 0:
  446.6 48.0 all-gather.2
  512.5 44.4 all-gather.4
